TPU v7x, 32 devices: a whole 2x2x4 slice. The times are simulated.
32 devices in a mesh: sp: 8 (over z, core), tp: 4 (over y, x).
Axes of the slice: x: 2, y: 2, z: 4, core: 2. Of those that a mesh axis runs over, the one named last changes fastest.
Arguments:
- queries: bfloat16 [2048, 1024], P('sp', 'tp'), may hold values from -250 to 250
- keys_values: bfloat16 [2, 2048, 256], P(None, 'sp'), may hold values from -8 to 8
- sink_logits: float32 [16], P('tp'), may hold values from 1 to 5
- proj_weight: bfloat16 [1024, 2048], P('tp'), may hold values from -0.75 to 0.75
- residual: bfloat16 [2048, 2048], P('sp', 'tp'), may hold values from -6 to 6
- norm_gain: float32 [2048], replicated, may hold values from 0.1 to 1.9
- routes: int32 [2048, 2], P('sp'), may hold values from 0 to 7, all different within a row; in each aligned block of 256 rows (0 to 255, 256 to 511, ...) at most 128 rows name the same one
- route_weights: float32 [2048, 2], P('sp'), may hold values from 0.2 to 1
- gate_weight: bfloat16 [8, 2048, 2048], P('sp', None, 'tp'), may hold values from -0.125 to 0.125
- up_weight: bfloat16 [8, 2048, 2048], P('sp', None, 'tp'), may hold values from -0.125 to 0.125
- down_weight: bfloat16 [8, 2048, 2048], P('sp', None, 'tp'), may hold values from -0.125 to 0.125
- shared_gate: bfloat16 [2048, 2048], P(None, 'tp'), may hold values from -0.125 to 0.125
- shared_up: bfloat16 [2048, 2048], P(None, 'tp'), may hold values from -0.125 to 0.125
- shared_down: bfloat16 [2048, 2048], P(None, 'tp'), may hold values from -0.125 to 0.125
Outputs:
- output: bfloat16 [2048, 2048], P('sp', 'tp')
Inputs may be any that keep to these rules, and one draw needn't show every extreme that they name: `routes`: the 2 experts of a position differ. In each aligned block of 256 positions no expert is named by more than 128 positions, and in some block one expert is named by exactly 128.
All inputs are finite; a program needn't handle non-finite values.
Results may differ from a plain program's by a relative error of at most 0.0067.
Values may be sent and summed in bfloat16 or wider, within the bound.
A program may use at most 64 MiB of HBM per device.

v0:
```python
import jax
import jax.numpy as jnp
from jax import lax
from jax.sharding import PartitionSpec as P

D = 2048
HEADS = 16
KV_HEADS = 4
HEAD_WIDTH = 64
WINDOW = 128
TOP_K = 2
EXP_DEV = 1
TOK_DEV = 256
norm_eps = 1e-06


def passed_along(value, axis, steps):
    count = lax.axis_size(axis)
    initial, last = (max(0, -steps), min(count, count - steps))
    return lax.ppermute(value, axis, [(source, source + steps) for source in range(initial, last)])


def per_device(
    queries,
    keys_values,
    sink_logits,
    proj_weight,
    residual,
    norm_gain,
    routes,
    route_weights,
    gate_weight,
    up_weight,
    down_weight,
    shared_gate,
    shared_up,
    shared_down,
):
    tp_index = lax.axis_index("tp")
    sp_index = lax.axis_index("sp")
    sp_count = lax.axis_size("sp")
    tp_count = lax.axis_size("tp")
    heads_here = sink_logits.shape[0]
    col_width = residual.shape[1]
    blocks = TOK_DEV // WINDOW
    kv_group = HEADS // KV_HEADS
    earlier_keys = passed_along(keys_values[:, TOK_DEV - WINDOW :, :], "sp", 1)
    extended = jnp.concatenate([earlier_keys, keys_values], axis=1)
    extended = extended.reshape(2, TOK_DEV + WINDOW, KV_HEADS, HEAD_WIDTH)
    head_ids = tp_index * heads_here + jnp.arange(heads_here, dtype=jnp.int32)
    chosen = jnp.take(extended, head_ids // kv_group, axis=2)
    earlier = chosen[:, :TOK_DEV].reshape(2, blocks, WINDOW, heads_here, HEAD_WIDTH)
    later = chosen[:, WINDOW:].reshape(2, blocks, WINDOW, heads_here, HEAD_WIDTH)
    banded = jnp.concatenate([earlier, later], axis=2)
    query_blocks = queries.reshape(blocks, WINDOW, heads_here, HEAD_WIDTH)
    score_matrix = jnp.einsum(
        "bqhd,bkhd->bhqk", query_blocks, banded[0], preferred_element_type=jnp.float32
    ) * HEAD_WIDTH ** (-0.5)
    query_pos = jnp.arange(WINDOW, dtype=jnp.int32)[:, None]
    key_pos = jnp.arange(2 * WINDOW, dtype=jnp.int32)[None, :]
    distance = WINDOW + query_pos - key_pos
    absolute = (
        sp_index * TOK_DEV
        + jnp.arange(blocks, dtype=jnp.int32)[:, None, None] * WINDOW
        - WINDOW
        + key_pos[None]
    )
    allowed = (distance >= 0)[None] & (distance < WINDOW)[None] & (absolute >= 0)
    masked = jnp.where(allowed[:, None], score_matrix, -jnp.inf)
    sink_value = sink_logits[None, :, None, None]
    highest = jnp.maximum(jnp.max(masked, axis=-1, keepdims=True), sink_value)
    weights_exp = jnp.exp(masked - highest)
    denominator = jnp.sum(weights_exp, axis=-1, keepdims=True) + jnp.exp(sink_value - highest)
    softmax_weights = (weights_exp / denominator).astype(jnp.bfloat16)
    attended_values = jnp.einsum(
        "bhqk,bkhd->bqhd", softmax_weights, banded[1], preferred_element_type=jnp.float32
    )
    attended_values = attended_values.astype(jnp.bfloat16).reshape(TOK_DEV, heads_here * HEAD_WIDTH)
    attended_all = lax.all_gather(attended_values, "tp", axis=1, tiled=True)
    weight_rows = proj_weight.shape[0]
    column_share = lax.all_to_all(
        proj_weight.reshape(weight_rows, tp_count, col_width),
        "tp",
        split_axis=1,
        concat_axis=0,
        tiled=True,
    )
    column_share = column_share.reshape(HEADS * HEAD_WIDTH, col_width)
    feature_sum = jnp.dot(attended_all, column_share, preferred_element_type=jnp.float32)
    stream_cols = (feature_sum + residual.astype(jnp.float32)).astype(jnp.bfloat16)
    stream_rows = lax.all_gather(stream_cols, "tp", axis=1, tiled=True)
    gate_eff = (norm_gain[None, :, None] * gate_weight.astype(jnp.float32)).astype(jnp.bfloat16)
    up_eff = (norm_gain[None, :, None] * up_weight.astype(jnp.float32)).astype(jnp.bfloat16)
    shared_gate_eff = (norm_gain[:, None] * shared_gate.astype(jnp.float32)).astype(jnp.bfloat16)
    shared_up_eff = (norm_gain[:, None] * shared_up.astype(jnp.float32)).astype(jnp.bfloat16)
    experts_total = EXP_DEV * sp_count
    capacity = 2 * TOK_DEV * TOP_K // experts_total
    rows_per_expert = sp_count * capacity
    flat_routes = routes.reshape(-1)
    onehot = (flat_routes[:, None] == jnp.arange(experts_total, dtype=jnp.int32)[None, :]).astype(
        jnp.int32
    )
    before = jnp.cumsum(onehot, axis=0) - onehot
    slot_rank = jnp.sum(before * onehot, axis=1)
    slot_index = (
        flat_routes % EXP_DEV * rows_per_expert + flat_routes // EXP_DEV * capacity + slot_rank
    )
    token_of = jnp.arange(TOK_DEV * TOP_K, dtype=jnp.int32) // TOP_K
    slot_owner = (
        jnp.full((EXP_DEV * rows_per_expert,), TOK_DEV, jnp.int32).at[slot_index].set(token_of)
    )
    picked_rows = jnp.take(stream_rows, slot_owner, axis=0, mode="fill", fill_value=0)
    arrived = lax.all_to_all(
        picked_rows.reshape(EXP_DEV, sp_count, capacity, stream_rows.shape[1]),
        "sp",
        split_axis=1,
        concat_axis=1,
        tiled=True,
    )
    arrived = arrived.reshape(EXP_DEV, rows_per_expert, D)
    routed_squares = jnp.sum(jnp.square(arrived.astype(jnp.float32)), axis=-1)
    gate_sum = jnp.einsum("erd,edf->erf", arrived, gate_eff, preferred_element_type=jnp.float32)
    up_sum = jnp.einsum("erd,edf->erf", arrived, up_eff, preferred_element_type=jnp.float32)
    own_squares = jnp.sum(jnp.square(stream_rows.astype(jnp.float32)), axis=-1)
    shared_gate_sum = jnp.dot(stream_rows, shared_gate_eff, preferred_element_type=jnp.float32)
    shared_up_sum = jnp.dot(stream_rows, shared_up_eff, preferred_element_type=jnp.float32)
    routed_scale = lax.rsqrt(routed_squares / D + norm_eps)[..., None]
    own_scale = lax.rsqrt(own_squares / D + norm_eps)[:, None]
    hidden = (jax.nn.silu(routed_scale * gate_sum) * (routed_scale * up_sum)).astype(jnp.bfloat16)
    shared_hidden = (jax.nn.silu(own_scale * shared_gate_sum) * (own_scale * shared_up_sum)).astype(
        jnp.bfloat16
    )
    routed_piece = lax.all_gather(hidden, "tp", axis=2, tiled=True)
    own_piece = lax.all_gather(shared_hidden[None], "tp", axis=2, tiled=True)
    expert_out = jnp.einsum(
        "erf,efd->erd", routed_piece, down_weight, preferred_element_type=jnp.float32
    )
    shared_out = jnp.dot(own_piece[0], shared_down, preferred_element_type=jnp.float32)
    outgoing = expert_out.astype(jnp.bfloat16).reshape(EXP_DEV, sp_count, capacity, col_width)
    returned = lax.all_to_all(outgoing, "sp", split_axis=1, concat_axis=1, tiled=True).reshape(
        EXP_DEV * rows_per_expert, col_width
    )
    picked = jnp.take(returned, slot_index, axis=0).reshape(TOK_DEV, TOP_K, col_width)
    routed_sum = jnp.einsum("nk,nkd->nd", route_weights, picked.astype(jnp.float32))
    return (stream_cols.astype(jnp.float32) + shared_out + routed_sum).astype(jnp.bfloat16)


def solution(mesh):
    placed = (
        P("sp", "tp"),
        P(None, "sp", None),
        P("tp"),
        P("tp", None),
        P("sp", "tp"),
        P(),
        P("sp", None),
        P("sp", None),
        P("sp", None, "tp"),
        P("sp", None, "tp"),
        P("sp", None, "tp"),
        P(None, "tp"),
        P(None, "tp"),
        P(None, "tp"),
    )
    return jax.shard_map(
        per_device, mesh=mesh, in_specs=placed, out_specs=P("sp", "tp"), check_vma=False
    )
```

profile of v0, /device:TPU:0, one launch (start us, length us, event | category | flops | bytes accessed | tf_op | source)
XLA Modules:
  0.0 293.3 jit_solution(9455327325811044780)
XLA Ops:
  6.5 1.2 copy.63
  7.8 3.2 %collective-permute-start = (bf16[2,128,256]{1,2,0:T(8,128)(2,1)S(1)}, bf16[2,128,256]{1,2,0:T(8,128)(2,1)}, u32[]{:S(2)}, u32[]{:S(2)}) collective-permute-start(bf16[2,128,256]{1,2,0:T(8,128)(2,1)S(1)} %slice.34), channel_id=1, source_target_pairs={{0,4},{4,8},{8,12},{12,16},{16,20},{20,24},{24,28},{1,5},{5,9},{9,... | collective-permute-start | bytes 393224 | tf_op jit(solution)/shard_map/ppermute | solution.py:20
  11.0 2.3 copy.73
  13.3 4.5 %all-to-all-start = ((bf16[256,4,512]{0,2,1:T(8,128)(2,1)}), bf16[256,4,512]{0,2,1:T(8,128)(2,1)S(1)}, u32[]{:S(2)}, u32[]{:S(2)}) async-start(bf16[256,4,512]{0,2,1:T(8,128)(2,1)} %bitcast.91), calls=%async_computation | async-start | bytes 2097152 | tf_op jit(solution)/shard_map/all_to_all | solution.py:81
  18.0 0.8 broadcast_and_fusion
  18.7 0.9 reshape.384
  19.6 1.0 pad_maximum_fusion
  20.7 1.4 gather_fusion
  22.0 1.1 select_bitcast_fusion
  23.2 0.8 fusion.47
  24.0 1.0 reshape.382
  25.1 0.8 copy_dynamic-update-slice_fusion.1
  25.8 1.0 reshape.383
  26.9 0.8 copy_dynamic-update-slice_fusion
  27.6 1.5 fusion.48
  29.2 0.2 fusion.29
  29.4 0.3 fusion.28
  30.0 12.7 %all_gather.12 = bf16[256,1024]{0,1:T(8,128)(2,1)} all-gather(bf16[256,256]{0,1:T(8,128)(2,1)S(1)} %bitcast.95), channel_id=1, replica_groups=mesh['sp'=8,'tp'=4] {'tp'}, dimensions={1}, use_global_device_ids=true | all-gather | bytes 655360 | tf_op jit(solution)/shard_map/all_gather | solution.py:79
  42.7 1.3 copy.74
  44.0 2.6 fusion.25
  46.8 0.1 eq.28
  47.0 0.1 reshape.334
  47.1 1.1 reduce-window.6
  48.3 0.2 slice_reduce_fusion
  48.7 0.2 mul.142
  48.9 2.4 scatter_custom_fusion
  51.4 20.4 %all-gather.6.cloned.1.call-done = bf16[256,2048]{1,0:T(8,128)(2,1)} async-done(((bf16[256,512]{1,0:T(8,128)(2,1)}), bf16[256,2048]{1,0:T(8,128)(2,1)}) %all-gather.6.cloned.1.call-update) | async-done | bytes 1048592 | tf_op jit(solution)/shard_map/all_gather | solution.py:91
  71.8 10.2 %gather_fusion.1 = bf16[1024,2048]{1,0:T(8,128)(2,1)} fusion(bf16[256,2048]{1,0:T(8,128)(2,1)} %all-gather.6.cloned.1.call-done, s32[1024]{0:T(1024)S(1)} %fusion.39), kind=kCustom, calls=%fused_computation.1 | custom fusion | bytes 8392704 | tf_op jit(solution)/shard_map/jit(_take)/gather | solution.py:112
  82.0 2.5 broadcast_select_fusion
  84.5 98.4 %all_to_all.25 = bf16[1,8,128,2048]{3,2,0,1:T(8,128)(2,1)S(1)} all-to-all(bf16[1,8,128,2048]{3,2,0,1:T(8,128)(2,1)S(1)} %broadcast_select_fusion), channel_id=1, replica_groups=mesh['sp'=8,'tp'=4] {'sp'}, dimensions={1} | all-to-all | bytes 8388608 | tf_op jit(solution)/shard_map/all_to_all | solution.py:113
  182.9 0.9 multiply_reduce_fusion
  183.8 0.7 copy-done.10
  184.5 2.4 fusion.3
  186.9 3.7 %multiply_convert_fusion.6 = bf16[1024,512]{1,0:T(8,128)(2,1)} fusion(f32[1024,512]{1,0:T(8,128)S(1)} %fusion.3, bf16[1024,2048]{1,0:T(8,128)(2,1)S(1)} %bitcast.89, bf16[1,2048,512]{2,1,0:T(8,128)(2,1)S(1)} %copy-done.11, f32[2048]{0:T(1024)S(1)} %copy-done.14, f32[1024]{0:T(1024)S(1)} %rsqrt_bitcast_fusion), kind=kOutput, calls=%fused_computation.18 | convolution fusion | flops 2154823680 | bytes 9449472 | tf_op jit(solution)/shard_map/erd,edf->erf/dot_general | solution.py:123
  190.7 0.3 multiply_reduce_fusion.1
  191.0 50.3 %all-gather.10.cloned.1.call-done = bf16[1024,2048]{1,0:T(8,128)(2,1)} async-done(((bf16[1024,512]{1,0:T(8,128)(2,1)}), bf16[1024,2048]{1,0:T(8,128)(2,1)}) %all-gather.10.cloned.1.call-update) | async-done | bytes 4194320 | tf_op jit(solution)/shard_map/all_gather | solution.py:133
  241.3 5.5 %fusion.16 = bf16[1024,512]{1,0:T(8,128)(2,1)} fusion(bf16[1024,2048]{1,0:T(8,128)(2,1)} %all-gather.10.cloned.1.call-done, bf16[1,2048,512]{2,1,0:T(8,128)(2,1)S(1)} %copy-done), kind=kOutput, calls=%fused_computation.24 | convolution fusion | flops 2148007936 | bytes 7340032 | tf_op jit(solution)/shard_map/erf,efd->erd/dot_general | solution.py:135
  246.8 4.6 %all-to-all-start.2 = ((bf16[1,8,128,512]{3,2,0,1:T(8,128)(2,1)}), bf16[1,8,128,512]{3,2,0,1:T(8,128)(2,1)}, u32[]{:S(2)}, u32[]{:S(2)}) async-start(bf16[1,8,128,512]{3,2,0,1:T(8,128)(2,1)} %bitcast.93), calls=%async_computation.2 | async-start | bytes 2097152 | tf_op jit(solution)/shard_map/all_to_all | solution.py:140
  251.4 2.6 fusion.23
  254.0 1.6 fusion.27
  255.6 0.1 reduce_sum.43
  255.9 0.2 copy.78
  256.1 0.2 copy.83
  256.3 21.8 %all-to-all-done.2 = bf16[1,8,128,512]{3,2,0,1:T(8,128)(2,1)} async-done(((bf16[1,8,128,512]{3,2,0,1:T(8,128)(2,1)}), bf16[1,8,128,512]{3,2,0,1:T(8,128)(2,1)}, u32[]{:S(2)}, u32[]{:S(2)}) %all-to-all-start.2) | async-done | bytes 1048608 | tf_op jit(solution)/shard_map/all_to_all | solution.py:140
  278.0 3.3 %gather_fusion.2 = bf16[512,512]{1,0:T(8,128)(2,1)S(1)} fusion(bf16[1024,512]{1,0:T(8,128)(2,1)} %bitcast.25, s32[1024]{0:T(1024)S(1)} %pad_clamp_fusion), kind=kCustom, calls=%fused_computation.2 | custom fusion | bytes 1050624 | tf_op jit(solution)/shard_map/jit(_take)/gather | solution.py:143
  281.4 0.2 gather.20
  281.6 1.8 fusion.30
  283.4 3.4 %fusion.26 = bf16[256,512]{1,0:T(8,128)(2,1)} fusion(bf16[256,2048]{1,0:T(8,128)(2,1)} %all-gather.8.cloned.1.call-done, bf16[2048,512]{1,0:T(8,128)(2,1)} %param.27, f32[256,1,512]{2,1,0:T(1,128)} %fusion.30, bf16[256,512]{1,0:T(8,128)(2,1)S(1)} %copy-done.3), kind=kOutput, calls=%fused_computation.35 | convolution fusion | flops 537395200 | bytes 4194304 | tf_op jit(solution)/shard_map/dot_general | solution.py:138
  (66 shorter events, 1.2 us)
Async XLA Ops:
  6.5 234.7 %copy-start = (bf16[1,2048,512]{2,1,0:T(8,128)(2,1)S(1)}, bf16[1,2048,512]{2,1,0:T(8,128)(2,1)}, u32[]{:S(2)}) copy-start(bf16[1,2048,512]{2,1,0:T(8,128)(2,1)} %param.24) | copy-start | bytes 6291460
  7.8 5.5 %copy-start.2 = (bf16[2,256,256]{1,2,0:T(8,128)(2,1)}, bf16[2,256,256]{1,2,0:T(8,128)(2,1)S(1)}, u32[]{:S(2)}) copy-start(bf16[2,256,256]{1,2,0:T(8,128)(2,1)S(1)} %copy.63) | copy-start | bytes 786436
  7.8 10.9 %copy-start.4 = (bf16[256,256]{1,0:T(8,128)(2,1)S(1)}, bf16[256,256]{1,0:T(8,128)(2,1)}, u32[]{:S(2)}) copy-start(bf16[256,256]{1,0:T(8,128)(2,1)} %param.14) | copy-start | bytes 393220
  7.8 11.8 %collective-permute-start = (bf16[2,128,256]{1,2,0:T(8,128)(2,1)S(1)}, bf16[2,128,256]{1,2,0:T(8,128)(2,1)}, u32[]{:S(2)}, u32[]{:S(2)}) collective-permute-start(bf16[2,128,256]{1,2,0:T(8,128)(2,1)S(1)} %slice.34), channel_id=1, source_target_pairs={{0,4},{4,8},{8,12},{12,16},{16,20},{20,24},{24,28},{1,5},{5,9},{9,... | collective-permute-start | bytes 393224 | tf_op jit(solution)/shard_map/ppermute | solution.py:20
  13.3 29.4 %all-to-all-start = ((bf16[256,4,512]{0,2,1:T(8,128)(2,1)}), bf16[256,4,512]{0,2,1:T(8,128)(2,1)S(1)}, u32[]{:S(2)}, u32[]{:S(2)}) async-start(bf16[256,4,512]{0,2,1:T(8,128)(2,1)} %bitcast.91), calls=%async_computation | async-start | bytes 2097152 | tf_op jit(solution)/shard_map/all_to_all | solution.py:81
  17.8 54.0 %all-gather.6.cloned.1.call-start = ((), (), s32[]{:S(2)}) async-start(), calls=%async_computation.3 | async-start | bytes 1310720 | tf_op jit(solution)/shard_map/all_gather | solution.py:91
  22.0 5.6 %copy-start.6 = (pred[2,128,256]{1,2,0:T(8,128)(4,1)S(1)}, pred[2,128,256]{1,2,0:T(8,128)(4,1)}, u32[]{:S(2)}) copy-start(pred[2,128,256]{1,2,0:T(8,128)(4,1)} %broadcast_and_fusion) | copy-start | bytes 196612
  24.0 5.1 %copy-start.9 = (f32[4]{0:T(128)S(1)}, f32[4]{0:T(128)}, u32[]{:S(2)}) copy-start(f32[4]{0:T(128)} %param.16) | copy-start | bytes 52
  27.6 1.8 copy-start.5
  29.8 14.3 %copy-start.13 = (bf16[256,512]{1,0:T(8,128)(2,1)S(1)}, bf16[256,512]{1,0:T(8,128)(2,1)}, u32[]{:S(2)}) copy-start(bf16[256,512]{1,0:T(8,128)(2,1)} %param.18) | copy-start | bytes 786436
  42.7 4.0 %copy-start.7 = (s32[256,2]{0,1:T(2,128)S(1)}, s32[256,2]{0,1:T(2,128)}, u32[]{:S(2)}) copy-start(s32[256,2]{0,1:T(2,128)} %param.20) | copy-start | bytes 6148
  46.6 194.7 %all-gather.10.cloned.1.call-start = ((), (), s32[]{:S(2)}) async-start(), calls=%async_computation.5 | async-start | bytes 5242880 | tf_op jit(solution)/shard_map/all_gather | solution.py:133
  182.9 1.6 copy-start.10
  182.9 1.6 copy-start.14
  184.5 2.4 copy-start.11
  186.9 3.8 %copy-start.1 = (bf16[256,2048]{1,0:T(8,128)(2,1)S(1)}, bf16[256,2048]{1,0:T(8,128)(2,1)}, u32[]{:S(2)}) copy-start(bf16[256,2048]{1,0:T(8,128)(2,1)} %all-gather.6.cloned.1.call-done) | copy-start | bytes 3145732
  246.8 31.3 %all-to-all-start.2 = ((bf16[1,8,128,512]{3,2,0,1:T(8,128)(2,1)}), bf16[1,8,128,512]{3,2,0,1:T(8,128)(2,1)}, u32[]{:S(2)}, u32[]{:S(2)}) async-start(bf16[1,8,128,512]{3,2,0,1:T(8,128)(2,1)} %bitcast.93), calls=%async_computation.2 | async-start | bytes 2097152 | tf_op jit(solution)/shard_map/all_to_all | solution.py:140
  251.4 32.0 %all-gather.8.cloned.1.call-start = ((), (), s32[]{:S(2)}) async-start(), calls=%async_computation.4 | async-start | bytes 1310720 | tf_op jit(solution)/shard_map/all_gather | solution.py:134
  251.4 2.6 copy-start.12
  254.0 2.1 copy-start.8
  281.6 1.8 copy-start.3
Sparse Core Ops, SparseCore 0:
  46.7 25.0 all-gather.5
  190.8 50.3 all-gather.9
  255.8 26.7 all-gather.7
where the time goes:
time: 294 us; the launch traced here: 293 us
  blocking collectives  111 us (38%)
  waiting for transfers between devices  92.4 us (31%)
  local copies, waits for them, and re-layouts  30.1 us (10%)
  matrix products  25.3 us (9%)
  between operations  13.5 us (5%)
  starting transfers between devices  12.4 us (4%)
  other arithmetic  8.46 us (3%)
    all_to_all x1, blocking collectives, per_device(): lax.all_to_all(picked_rows.reshape(EXP_DEV, sp_count, capacity, stream_ro...  98.4 us
    all_gather x1, waiting for transfers between devices, per_device(): routed_piece = lax.all_gather(hidden, 'tp', axis=2, tiled=True)  50.3 us
    all_to_all x1, waiting for transfers between devices, per_device(): lax.all_to_all(outgoing, 'sp', split_axis=1, concat_axis=1, tiled=True)  21.8 us
    all_gather x1, waiting for transfers between devices, per_device(): stream_rows = lax.all_gather(stream_cols, 'tp', axis=1, tiled=True)  20.4 us
    all_gather x1, blocking collectives, per_device(): attended_all = lax.all_gather(attended_values, 'tp', axis=1, tiled=True)  12.7 us
    gather x1, local copies, waits for them, and re-layouts, per_device(): jnp.take(stream_rows, slot_owner, axis=0, mode='fill', fill_value=0)  10.2 us
  transfers between devices with their start and end apart: 6, of which 3 were waited for; matrix products, arithmetic and copies ran while one was open for 10% of the time, Pallas kernels for 0%

commit v1 on v0

--- a/solution.py
+++ b/solution.py
@@ -130,11 +130,39 @@
     shared_hidden = (jax.nn.silu(own_scale * shared_gate_sum) * (own_scale * shared_up_sum)).astype(
         jnp.bfloat16
     )
-    routed_piece = lax.all_gather(hidden, "tp", axis=2, tiled=True)
     own_piece = lax.all_gather(shared_hidden[None], "tp", axis=2, tiled=True)
-    expert_out = jnp.einsum(
-        "erf,efd->erd", routed_piece, down_weight, preferred_element_type=jnp.float32
+    devices, index, extent = (lax.axis_size("tp"), lax.axis_index("tp"), hidden.shape[2])
+    right = [(i, (i + 1) % devices) for i in range(devices)]
+    behind = [(i, (i - 1) % devices) for i in range(devices)]
+    half = devices // 2
+    from_left = from_right = hidden
+    total = jnp.einsum(
+        "erf,efd->erd",
+        hidden,
+        lax.dynamic_slice_in_dim(down_weight, index * extent, hidden.shape[2], axis=1),
+        preferred_element_type=jnp.float32,
     )
+    for turn in range(1, half + 1):
+        from_left = lax.ppermute(from_left, "tp", right)
+        if turn < devices - half:
+            from_right = lax.ppermute(from_right, "tp", behind)
+            total = total + jnp.einsum(
+                "erf,efd->erd",
+                from_right,
+                lax.dynamic_slice_in_dim(
+                    down_weight, (index + turn) % devices * extent, from_right.shape[2], axis=1
+                ),
+                preferred_element_type=jnp.float32,
+            )
+        total = total + jnp.einsum(
+            "erf,efd->erd",
+            from_left,
+            lax.dynamic_slice_in_dim(
+                down_weight, (index - turn) % devices * extent, from_left.shape[2], axis=1
+            ),
+            preferred_element_type=jnp.float32,
+        )
+    expert_out = total
     shared_out = jnp.dot(own_piece[0], shared_down, preferred_element_type=jnp.float32)
     outgoing = expert_out.astype(jnp.bfloat16).reshape(EXP_DEV, sp_count, capacity, col_width)
     returned = lax.all_to_all(outgoing, "sp", split_axis=1, concat_axis=1, tiled=True).reshape(

time: 294 us -> 310 us (1.054)
  waiting for transfers between devices: 92.4 us -> 103 us
    ppermute x0 -> x3, waiting for transfers between devices: none -> 61 us  [the longest x2 43 us: per_device(): from_left = lax.ppermute(from_left, 'tp', right)]
    all_gather x1 -> x0, waiting for transfers between devices: 50.3 us -> none  [per_device(): routed_piece = lax.all_gather(hidden, 'tp', axis=2, tiled=True)]
    ppermute x0 -> x3, starting transfers between devices: none -> 3.49 us  [the longest x2 2.04 us: per_device(): from_left = lax.ppermute(from_left, 'tp', right)]
    dot_general x1 -> x4, matrix products: 5.49 us -> 7.49 us  [the longest x2 3.63 us: per_device(): jnp.einsum('erf,efd->erd', from_left, lax.dynamic_slice_in_dim(down_weigh...]
  transfers between devices with their start and end apart: 6 -> 8, of which waited for: 3 -> 5; matrix products, arithmetic and copies ran while one was open for 10% -> 11% of each run, Pallas kernels for 0% -> 0%
where the time goes in v1:
time: 310 us; the launch traced here: 309 us
  blocking collectives  111 us (36%)
  waiting for transfers between devices  103 us (33%)
  local copies, waits for them, and re-layouts  30.1 us (10%)
  matrix products  27.3 us (9%)
  starting transfers between devices  15.5 us (5%)
  between operations  13.8 us (4%)
  other arithmetic  8.46 us (3%)
    all_to_all x1, blocking collectives, per_device(): lax.all_to_all(picked_rows.reshape(EXP_DEV, sp_count, capacity, stream_ro...  98.4 us
    ppermute x2, waiting for transfers between devices, per_device(): from_left = lax.ppermute(from_left, 'tp', right)  43 us
    all_to_all x1, waiting for transfers between devices, per_device(): lax.all_to_all(outgoing, 'sp', split_axis=1, concat_axis=1, tiled=True)  21.7 us
    all_gather x1, waiting for transfers between devices, per_device(): stream_rows = lax.all_gather(stream_cols, 'tp', axis=1, tiled=True)  20.4 us
    ppermute x1, waiting for transfers between devices, per_device(): from_right = lax.ppermute(from_right, 'tp', behind)  18 us
    all_gather x1, blocking collectives, per_device(): attended_all = lax.all_gather(attended_values, 'tp', axis=1, tiled=True)  12.7 us
    gather x1, local copies, waits for them, and re-layouts, per_device(): jnp.take(stream_rows, slot_owner, axis=0, mode='fill', fill_value=0)  10.2 us
  transfers between devices with their start and end apart: 8, of which 5 were waited for; matrix products, arithmetic and copies ran while one was open for 11% of the time, Pallas kernels for 0%

profile of v1, /device:TPU:0, one launch (start us, length us, event | category | flops | bytes accessed | tf_op | source)
XLA Modules:
  0.0 309.3 jit_solution(376400494426715132)
XLA Ops:
  6.5 1.2 copy.63
  7.8 3.2 %collective-permute-start = (bf16[2,128,256]{1,2,0:T(8,128)(2,1)S(1)}, bf16[2,128,256]{1,2,0:T(8,128)(2,1)}, u32[]{:S(2)}, u32[]{:S(2)}) collective-permute-start(bf16[2,128,256]{1,2,0:T(8,128)(2,1)S(1)} %slice.34), channel_id=1, source_target_pairs={{0,4},{4,8},{8,12},{12,16},{16,20},{20,24},{24,28},{1,5},{5,9},{9,... | collective-permute-start | bytes 393224 | tf_op jit(solution)/shard_map/ppermute | solution.py:20
  11.0 2.3 copy.73
  13.3 4.5 %all-to-all-start = ((bf16[256,4,512]{0,2,1:T(8,128)(2,1)}), bf16[256,4,512]{0,2,1:T(8,128)(2,1)S(1)}, u32[]{:S(2)}, u32[]{:S(2)}) async-start(bf16[256,4,512]{0,2,1:T(8,128)(2,1)} %bitcast.109), calls=%async_computation | async-start | bytes 2097152 | tf_op jit(solution)/shard_map/all_to_all | solution.py:81
  18.0 0.8 broadcast_and_fusion
  18.7 0.9 reshape.410
  19.6 1.0 pad_maximum_fusion
  20.7 1.4 gather_fusion
  22.0 1.1 select_bitcast_fusion
  23.2 0.8 fusion.60
  24.0 1.0 reshape.408
  25.1 0.8 copy_dynamic-update-slice_fusion.1
  25.8 1.0 reshape.409
  26.9 0.8 copy_dynamic-update-slice_fusion
  27.6 1.5 fusion.61
  29.4 0.3 fusion.23
  30.0 12.7 %all_gather.9 = bf16[256,1024]{0,1:T(8,128)(2,1)} all-gather(bf16[256,256]{0,1:T(8,128)(2,1)S(1)} %bitcast.112), channel_id=1, replica_groups=mesh['sp'=8,'tp'=4] {'tp'}, dimensions={1}, use_global_device_ids=true | all-gather | bytes 655360 | tf_op jit(solution)/shard_map/all_gather | solution.py:79
  42.7 1.3 copy.74
  44.0 2.6 fusion.20
  47.1 1.1 reduce-window.6
  48.2 0.2 slice_reduce_fusion
  48.9 2.4 scatter_custom_fusion
  51.4 20.4 %all-gather.4.cloned.1.call-done = bf16[256,2048]{1,0:T(8,128)(2,1)} async-done(((bf16[256,512]{1,0:T(8,128)(2,1)}), bf16[256,2048]{1,0:T(8,128)(2,1)}) %all-gather.4.cloned.1.call-update) | async-done | bytes 1048592 | tf_op jit(solution)/shard_map/all_gather | solution.py:91
  71.8 10.2 %gather_fusion.1 = bf16[1024,2048]{1,0:T(8,128)(2,1)} fusion(bf16[256,2048]{1,0:T(8,128)(2,1)} %all-gather.4.cloned.1.call-done, s32[1024]{0:T(1024)S(1)} %fusion.48), kind=kCustom, calls=%fused_computation.1 | custom fusion | bytes 8392704 | tf_op jit(solution)/shard_map/jit(_take)/gather | solution.py:112
  81.9 2.5 broadcast_select_fusion
  84.5 98.4 %all_to_all.25 = bf16[1,8,128,2048]{3,2,0,1:T(8,128)(2,1)S(1)} all-to-all(bf16[1,8,128,2048]{3,2,0,1:T(8,128)(2,1)S(1)} %broadcast_select_fusion), channel_id=1, replica_groups=mesh['sp'=8,'tp'=4] {'sp'}, dimensions={1} | all-to-all | bytes 8388608 | tf_op jit(solution)/shard_map/all_to_all | solution.py:113
  182.9 0.9 multiply_reduce_fusion
  183.8 0.7 copy-done.10
  184.5 2.4 fusion.3
  186.9 3.8 %multiply_convert_fusion.6 = bf16[1024,512]{1,0:T(8,128)(2,1)} fusion(f32[1024,512]{1,0:T(8,128)S(1)} %fusion.3, bf16[1024,2048]{1,0:T(8,128)(2,1)S(1)} %bitcast.106, bf16[1,2048,512]{2,1,0:T(8,128)(2,1)S(1)} %copy-done.11, f32[2048]{0:T(1024)S(1)} %copy-done.14, f32[1024]{0:T(1024)S(1)} %rsqrt_bitcast_fusion), kind=kOutput, calls=%fused_computation.17 | convolution fusion | flops 2154823680 | bytes 9449472 | tf_op jit(solution)/shard_map/erd,edf->erf/dot_general | solution.py:123
  190.7 1.5 collective-permute-start.2
  192.1 1.5 collective-permute-start.1
  193.6 0.3 multiply_reduce_fusion.1
  193.9 24.0 %collective-permute-done.2 = bf16[1,1024,512]{2,1,0:T(8,128)(2,1)} collective-permute-done((bf16[1,1024,512]{2,1,0:T(8,128)(2,1)}, bf16[1,1024,512]{2,1,0:T(8,128)(2,1)}, u32[]{:S(2)}, u32[]{:S(2)}) %collective-permute-start.2) | collective-permute-done | bytes 1048608 | tf_op jit(solution)/shard_map/ppermute | solution.py:146
  217.9 0.6 collective-permute-start.3
  218.5 1.9 fusion.33
  220.4 1.9 fusion.25
  222.4 18.0 %collective-permute-done.1 = bf16[1,1024,512]{2,1,0:T(8,128)(2,1)} collective-permute-done((bf16[1,1024,512]{2,1,0:T(8,128)(2,1)}, bf16[1,1024,512]{2,1,0:T(8,128)(2,1)}, u32[]{:S(2)}, u32[]{:S(2)}) %collective-permute-start.1) | collective-permute-done | bytes 1048608 | tf_op jit(solution)/shard_map/ppermute | solution.py:148
  240.4 1.9 fusion.27
  242.3 18.9 %collective-permute-done.3 = bf16[1,1024,512]{2,1,0:T(8,128)(2,1)S(1)} collective-permute-done((bf16[1,1024,512]{2,1,0:T(8,128)(2,1)}, bf16[1,1024,512]{2,1,0:T(8,128)(2,1)S(1)}, u32[]{:S(2)}, u32[]{:S(2)}) %collective-permute-start.3) | collective-permute-done | bytes 1048608 | tf_op jit(solution)/shard_map/ppermute | solution.py:146
  261.3 1.7 add_convert_fusion
  263.0 4.2 %all-to-all-start.2 = ((bf16[1,8,128,512]{3,2,0,1:T(8,128)(2,1)}), bf16[1,8,128,512]{3,2,0,1:T(8,128)(2,1)}, u32[]{:S(2)}, u32[]{:S(2)}) async-start(bf16[1,8,128,512]{3,2,0,1:T(8,128)(2,1)} %bitcast.107), calls=%async_computation.2 | async-start | bytes 2097152 | tf_op jit(solution)/shard_map/all_to_all | solution.py:168
  267.3 2.6 fusion.18
  269.9 1.6 fusion.22
  272.1 21.7 %all-to-all-done.2 = bf16[1,8,128,512]{3,2,0,1:T(8,128)(2,1)} async-done(((bf16[1,8,128,512]{3,2,0,1:T(8,128)(2,1)}), bf16[1,8,128,512]{3,2,0,1:T(8,128)(2,1)}, u32[]{:S(2)}, u32[]{:S(2)}) %all-to-all-start.2) | async-done | bytes 1048608 | tf_op jit(solution)/shard_map/all_to_all | solution.py:168
  293.8 3.3 %gather_fusion.2 = bf16[512,512]{1,0:T(8,128)(2,1)S(1)} fusion(bf16[1024,512]{1,0:T(8,128)(2,1)} %bitcast.32, s32[1024]{0:T(1024)S(1)} %pad_clamp_fusion), kind=kCustom, calls=%fused_computation.2 | custom fusion | bytes 1050624 | tf_op jit(solution)/shard_map/jit(_take)/gather | solution.py:171
  297.3 1.8 fusion.39
  299.1 3.4 %fusion.21 = bf16[256,512]{1,0:T(8,128)(2,1)} fusion(bf16[256,2048]{1,0:T(8,128)(2,1)} %all-gather.6.cloned.1.call-done, bf16[2048,512]{1,0:T(8,128)(2,1)} %param.27, f32[256,1,512]{2,1,0:T(1,128)} %fusion.39, bf16[256,512]{1,0:T(8,128)(2,1)S(1)} %copy-done.3), kind=kOutput, calls=%fused_computation.33 | convolution fusion | flops 537395200 | bytes 4194304 | tf_op jit(solution)/shard_map/dot_general | solution.py:166
  (72 shorter events, 2.5 us)
Async XLA Ops:
  6.5 212.0 %copy-start = (bf16[1,2048,512]{2,1,0:T(8,128)(2,1)S(1)}, bf16[1,2048,512]{2,1,0:T(8,128)(2,1)}, u32[]{:S(2)}) copy-start(bf16[1,2048,512]{2,1,0:T(8,128)(2,1)} %param.24) | copy-start | bytes 6291460
  7.8 5.5 %copy-start.2 = (bf16[2,256,256]{1,2,0:T(8,128)(2,1)}, bf16[2,256,256]{1,2,0:T(8,128)(2,1)S(1)}, u32[]{:S(2)}) copy-start(bf16[2,256,256]{1,2,0:T(8,128)(2,1)S(1)} %copy.63) | copy-start | bytes 786436
  7.8 10.9 %copy-start.4 = (bf16[256,256]{1,0:T(8,128)(2,1)S(1)}, bf16[256,256]{1,0:T(8,128)(2,1)}, u32[]{:S(2)}) copy-start(bf16[256,256]{1,0:T(8,128)(2,1)} %param.14) | copy-start | bytes 393220
  7.8 11.8 %collective-permute-start = (bf16[2,128,256]{1,2,0:T(8,128)(2,1)S(1)}, bf16[2,128,256]{1,2,0:T(8,128)(2,1)}, u32[]{:S(2)}, u32[]{:S(2)}) collective-permute-start(bf16[2,128,256]{1,2,0:T(8,128)(2,1)S(1)} %slice.34), channel_id=1, source_target_pairs={{0,4},{4,8},{8,12},{12,16},{16,20},{20,24},{24,28},{1,5},{5,9},{9,... | collective-permute-start | bytes 393224 | tf_op jit(solution)/shard_map/ppermute | solution.py:20
  13.3 29.4 %all-to-all-start = ((bf16[256,4,512]{0,2,1:T(8,128)(2,1)}), bf16[256,4,512]{0,2,1:T(8,128)(2,1)S(1)}, u32[]{:S(2)}, u32[]{:S(2)}) async-start(bf16[256,4,512]{0,2,1:T(8,128)(2,1)} %bitcast.109), calls=%async_computation | async-start | bytes 2097152 | tf_op jit(solution)/shard_map/all_to_all | solution.py:81
  17.8 54.0 %all-gather.4.cloned.1.call-start = ((), (), s32[]{:S(2)}) async-start(), calls=%async_computation.3 | async-start | bytes 1310720 | tf_op jit(solution)/shard_map/all_gather | solution.py:91
  22.0 5.6 %copy-start.6 = (pred[2,128,256]{1,2,0:T(8,128)(4,1)S(1)}, pred[2,128,256]{1,2,0:T(8,128)(4,1)}, u32[]{:S(2)}) copy-start(pred[2,128,256]{1,2,0:T(8,128)(4,1)} %broadcast_and_fusion) | copy-start | bytes 196612
  24.0 5.1 %copy-start.9 = (f32[4]{0:T(128)S(1)}, f32[4]{0:T(128)}, u32[]{:S(2)}) copy-start(f32[4]{0:T(128)} %param.16) | copy-start | bytes 52
  27.6 1.8 copy-start.5
  29.8 14.3 %copy-start.13 = (bf16[256,512]{1,0:T(8,128)(2,1)S(1)}, bf16[256,512]{1,0:T(8,128)(2,1)}, u32[]{:S(2)}) copy-start(bf16[256,512]{1,0:T(8,128)(2,1)} %param.18) | copy-start | bytes 786436
  42.7 3.9 %copy-start.7 = (s32[256,2]{0,1:T(2,128)S(1)}, s32[256,2]{0,1:T(2,128)}, u32[]{:S(2)}) copy-start(s32[256,2]{0,1:T(2,128)} %param.20) | copy-start | bytes 6148
  182.9 1.6 copy-start.10
  182.9 1.6 copy-start.14
  184.5 2.4 copy-start.11
  186.9 6.7 %copy-start.1 = (bf16[256,2048]{1,0:T(8,128)(2,1)S(1)}, bf16[256,2048]{1,0:T(8,128)(2,1)}, u32[]{:S(2)}) copy-start(bf16[256,2048]{1,0:T(8,128)(2,1)} %all-gather.4.cloned.1.call-done) | copy-start | bytes 3145732
  190.7 27.2 %collective-permute-start.2 = (bf16[1,1024,512]{2,1,0:T(8,128)(2,1)}, bf16[1,1024,512]{2,1,0:T(8,128)(2,1)}, u32[]{:S(2)}, u32[]{:S(2)}) collective-permute-start(bf16[1,1024,512]{2,1,0:T(8,128)(2,1)} %bitcast.23), channel_id=1, source_target_pairs={{0,1},{1,2},{2,3},{3,0},{4,5},{5,6},{6,7},{7,4},{8,9},{9,10},{10,1... | collective-permute-start | bytes 3145736 | tf_op jit(solution)/shard_map/ppermute | solution.py:146
  192.1 48.3 %collective-permute-start.1 = (bf16[1,1024,512]{2,1,0:T(8,128)(2,1)}, bf16[1,1024,512]{2,1,0:T(8,128)(2,1)}, u32[]{:S(2)}, u32[]{:S(2)}) collective-permute-start(bf16[1,1024,512]{2,1,0:T(8,128)(2,1)} %bitcast.23), channel_id=1, source_target_pairs={{0,3},{1,0},{2,1},{3,2},{4,7},{5,4},{6,5},{7,6},{8,11},{9,8},{10,9... | collective-permute-start | bytes 3145736 | tf_op jit(solution)/shard_map/ppermute | solution.py:148
  217.9 43.3 %collective-permute-start.3 = (bf16[1,1024,512]{2,1,0:T(8,128)(2,1)}, bf16[1,1024,512]{2,1,0:T(8,128)(2,1)S(1)}, u32[]{:S(2)}, u32[]{:S(2)}) collective-permute-start(bf16[1,1024,512]{2,1,0:T(8,128)(2,1)} %collective-permute-done.2), channel_id=1, source_target_pairs={{0,1},{1,2},{2,3},{3,0},{4,5},{5,6},{6,7},{7,4},{8,9},{9,10},{10,1... | collective-permute-start | bytes 3145736 | tf_op jit(solution)/shard_map/ppermute | solution.py:146
  263.0 30.8 %all-to-all-start.2 = ((bf16[1,8,128,512]{3,2,0,1:T(8,128)(2,1)}), bf16[1,8,128,512]{3,2,0,1:T(8,128)(2,1)}, u32[]{:S(2)}, u32[]{:S(2)}) async-start(bf16[1,8,128,512]{3,2,0,1:T(8,128)(2,1)} %bitcast.107), calls=%async_computation.2 | async-start | bytes 2097152 | tf_op jit(solution)/shard_map/all_to_all | solution.py:168
  267.2 31.9 %all-gather.6.cloned.1.call-start = ((), (), s32[]{:S(2)}) async-start(), calls=%async_computation.4 | async-start | bytes 1310720 | tf_op jit(solution)/shard_map/all_gather | solution.py:133
  267.3 2.6 copy-start.12
  269.8 2.1 copy-start.8
  297.3 1.8 copy-start.3
Sparse Core Ops, SparseCore 0:
  46.7 24.9 all-gather.3
  271.6 26.6 all-gather.5
